TPU v7x, 32 devices: a whole 2x2x4 slice. The times are simulated.
32 devices in a mesh: ep: 8 (over z, y), tp: 4 (over x, core).
Axes of the slice: x: 2, y: 2, z: 4, core: 2. Of those that a mesh axis runs over, the one named last changes fastest.
Arguments:
- resid: bfloat16 [256, 2048], P('ep'), may hold values from -6 to 6
- mix_gain: bfloat16 [2048], replicated, may hold values from 0.099609375 to 1.8984375
- proj_x: bfloat16 [2048, 512], P(None, 'tp'), may hold values from -0.125 to 0.125
- proj_z: bfloat16 [2048, 512], P(None, 'tp'), may hold values from -0.125 to 0.125
- proj_b: bfloat16 [2048, 512], P(None, 'tp'), may hold values from -0.125 to 0.125
- proj_c: bfloat16 [2048, 512], P(None, 'tp'), may hold values from -0.125 to 0.125
- proj_step: bfloat16 [2048, 8], replicated, may hold values from -0.125 to 0.125
- step_bias: float32 [8], P('tp'), may hold values from -5 to -1
- decay_rate: float32 [8], P('tp'), may hold values from 1 to 16
- conv_taps: bfloat16 [3, 4, 512], P(None, None, 'tp'), may hold values from -3 to 3
- conv_state: bfloat16 [256, 3, 3, 512], P('ep', None, None, 'tp'), may hold values from -6 to 6
- scan_state: float32 [256, 8, 64, 128], P('ep', 'tp'), may hold values from -2.5 to 2.5
- inner_gain: bfloat16 [512], P('tp'), may hold values from 0.099609375 to 1.8984375
- proj_out: bfloat16 [512, 2048], P('tp'), may hold values from -0.25 to 0.25
- post_gain: bfloat16 [2048], replicated, may hold values from 0.099609375 to 1.8984375
- ffn_gain: bfloat16 [2048], replicated, may hold values from 0.099609375 to 1.8984375
- group_router: bfloat16 [2048, 2], replicated, may hold values from -0.125 to 0.125
- expert_router: bfloat16 [2048, 8], replicated, may hold values from -0.125 to 0.125
- route_experts: int32 [256, 4], P('ep'), may hold values from 0 to 7, as said below
- expert_gate: bfloat16 [8, 2048, 1024], P('ep', None, 'tp'), may hold values from -0.125 to 0.125
- expert_up: bfloat16 [8, 2048, 1024], P('ep', None, 'tp'), may hold values from -0.125 to 0.125
- expert_down: bfloat16 [8, 1024, 2048], P('ep', 'tp')
- dense_switch: bfloat16 [2048], replicated, may hold values from -0.125 to 0.125
- dense_gate: bfloat16 [2048, 2048], P('ep', 'tp'), may hold values from -0.125 to 0.125
- dense_up: bfloat16 [2048, 2048], P('ep', 'tp'), may hold values from -0.125 to 0.125
- dense_down: bfloat16 [2048, 2048], P('ep', 'tp')
- out_gain: bfloat16 [2048], P('tp'), may hold values from 0.099609375 to 1.8984375
Outputs:
- layer_out: bfloat16 [256, 2048], P('ep', 'tp')
- new_state: float32 [256, 8, 64, 128], P('ep', 'tp')
- new_conv: bfloat16 [256, 3, 3, 512], P('ep', None, None, 'tp')
Inputs may be any that keep to these rules, and one draw needn't show every extreme that they name: `route_experts`: each row names 4 different experts, all from one group of 4 consecutive expert numbers. Within each aligned block of 32 rows (the rows of one index of ep) no expert is named more than 32 times, and one expert, the same in every block, is named exactly 32 times in every block.
All inputs are finite; a program needn't handle non-finite values.
Results may differ from a plain program's by a relative error of at most 0.019.
Values may be sent and summed in bfloat16 or wider, within the bound.
A program may use at most 64 MiB of HBM per device.

v0:
```python
import jax
import jax.numpy as jnp
from jax import lax
from jax.sharding import PartitionSpec as P

norm_eps = 1e-06


def scaled_rows(values, gain):
    values = values.astype(jnp.float32)
    mean_square = jnp.mean(values * values, axis=-1, keepdims=True)
    return values * lax.rsqrt(mean_square + norm_eps) * gain.astype(jnp.float32)


def softmax_plain(logits):
    weights = jnp.exp(logits)
    return weights / jnp.sum(weights, axis=-1, keepdims=True)


def on_device(
    resid,
    mix_gain,
    proj_x,
    proj_z,
    proj_b,
    proj_c,
    proj_step,
    step_bias,
    decay_rate,
    conv_taps,
    conv_state,
    scan_state,
    inner_gain,
    proj_out,
    post_gain,
    ffn_gain,
    group_router,
    expert_router,
    route_experts,
    expert_gate,
    expert_up,
    expert_down,
    dense_switch,
    dense_gate,
    dense_up,
    dense_down,
    out_gain,
):
    tp_index = lax.axis_index("tp")
    seqs = resid.shape[0]
    width = resid.shape[1]
    quarter = width // lax.axis_size("tp")
    heads_here = scan_state.shape[1]
    head_dim = scan_state.shape[2]
    state_dim = scan_state.shape[3]
    channels = conv_state.shape[3]
    repeat = heads_here // (channels // state_dim)
    normed = scaled_rows(resid, mix_gain).astype(jnp.bfloat16)
    fresh = jnp.stack(
        [
            jnp.dot(normed, proj_x, preferred_element_type=jnp.float32),
            jnp.dot(normed, proj_b, preferred_element_type=jnp.float32),
            jnp.dot(normed, proj_c, preferred_element_type=jnp.float32),
        ],
        axis=1,
    ).astype(jnp.bfloat16)
    gate_z = jnp.dot(normed, proj_z, preferred_element_type=jnp.float32)
    step_all = jnp.dot(normed, proj_step, preferred_element_type=jnp.float32)
    step_raw = lax.dynamic_slice_in_dim(step_all, tp_index * heads_here, heads_here, 1)
    history = jnp.concatenate([conv_state, fresh[:, :, None, :]], axis=2)
    activated = jax.nn.silu(
        jnp.sum(history.astype(jnp.float32) * conv_taps.astype(jnp.float32)[None], axis=2)
    )
    xs_heads = activated[:, 0].reshape(seqs, heads_here, head_dim)
    b_heads = jnp.repeat(activated[:, 1].reshape(seqs, -1, state_dim), repeat, axis=1)
    c_heads = jnp.repeat(activated[:, 2].reshape(seqs, -1, state_dim), repeat, axis=1)
    step = jax.nn.softplus(step_raw + step_bias)
    keep = jnp.exp(-decay_rate * step)
    driven = step[:, :, None] * xs_heads
    new_state = keep[:, :, None, None] * scan_state + driven[:, :, :, None] * b_heads[:, :, None, :]
    read = jnp.sum(new_state * c_heads[:, :, None, :], axis=3).reshape(seqs, channels)
    gated = (read * jax.nn.silu(gate_z) * inner_gain.astype(jnp.float32)).astype(jnp.bfloat16)
    mixed = lax.psum(
        jnp.dot(gated, proj_out, preferred_element_type=jnp.float32).astype(jnp.bfloat16), "tp"
    ).astype(jnp.float32)
    stream = (resid.astype(jnp.float32) + scaled_rows(mixed, post_gain)).astype(jnp.bfloat16)
    feed = scaled_rows(stream, ffn_gain).astype(jnp.bfloat16)
    feed_quarter = lax.dynamic_slice_in_dim(feed, tp_index * quarter, quarter, 1)
    expert_count = expert_router.shape[1]
    group_size = expert_count // group_router.shape[1]
    pick_count = route_experts.shape[1]
    group_prob = softmax_plain(jnp.dot(feed, group_router, preferred_element_type=jnp.float32))
    expert_logits = jnp.dot(feed, expert_router, preferred_element_type=jnp.float32)
    matches = route_experts[:, :, None] == jnp.arange(expert_count, dtype=jnp.int32)[None, None, :]
    pick_logits = jnp.sum(jnp.where(matches, expert_logits[:, None, :], 0.0), axis=2)
    chosen_group = route_experts[:, 0] // group_size
    group_ids = jnp.arange(group_router.shape[1], dtype=jnp.int32)
    group_weight = jnp.sum(
        jnp.where(chosen_group[:, None] == group_ids[None, :], group_prob, 0.0), axis=1
    )
    pick_weight = softmax_plain(pick_logits) * group_weight[:, None]
    capacity = 2 * seqs * pick_count // expert_count
    flat_picks = route_experts.reshape(-1)
    one_hot = (flat_picks[:, None] == jnp.arange(expert_count, dtype=jnp.int32)[None, :]).astype(
        jnp.int32
    )
    slot = jnp.sum((jnp.cumsum(one_hot, axis=0) - one_hot) * one_hot, axis=1)
    target = flat_picks * capacity + slot
    repeated = jnp.repeat(feed, pick_count, axis=0)
    outgoing = jnp.zeros((expert_count * capacity, width), jnp.bfloat16).at[target].set(repeated)
    outgoing = outgoing.reshape(expert_count, capacity, width)
    arrived = lax.all_to_all(outgoing, "ep", split_axis=0, concat_axis=0, tiled=True)
    sources = arrived.shape[0]
    items = arrived.shape[1]
    rows = arrived.reshape(sources * items, width)
    gate_value = jnp.dot(rows, expert_gate[0], preferred_element_type=jnp.float32)
    up_value = jnp.dot(rows, expert_up[0], preferred_element_type=jnp.float32)
    hidden = (jax.nn.silu(gate_value) * up_value).astype(jnp.bfloat16)
    result = jnp.dot(hidden, expert_down[0], preferred_element_type=jnp.float32).reshape(
        sources, items, width
    )
    summed = lax.psum_scatter(result.astype(jnp.bfloat16), "tp", scatter_dimension=2, tiled=True)
    returned = lax.all_to_all(summed, "ep", split_axis=0, concat_axis=0, tiled=True)
    fetched = returned.reshape(expert_count * capacity, quarter)[target].reshape(
        seqs, pick_count, quarter
    )
    routed = jnp.sum(fetched.astype(jnp.float32) * pick_weight[:, :, None], axis=1)
    gate_piece = jnp.einsum(
        "sd,cd->sc",
        feed_quarter,
        lax.all_gather(dense_gate, "ep", axis=0, tiled=True),
        preferred_element_type=jnp.float32,
    )
    up_piece = jnp.einsum(
        "sd,cd->sc",
        feed_quarter,
        lax.all_gather(dense_up, "ep", axis=0, tiled=True),
        preferred_element_type=jnp.float32,
    )
    gate_sum = gate_piece
    up_sum = up_piece
    gate_sum, up_sum = (
        lax.psum(gate_sum.astype(jnp.bfloat16), "tp").astype(jnp.float32),
        lax.psum(up_sum.astype(jnp.bfloat16), "tp").astype(jnp.float32),
    )
    dense_hidden = (jax.nn.silu(gate_sum) * up_sum).astype(jnp.bfloat16)
    dense_out = jnp.dot(
        dense_hidden,
        lax.all_gather(dense_down, "ep", axis=0, tiled=True),
        preferred_element_type=jnp.float32,
    )
    switch = jax.nn.sigmoid(jnp.dot(feed, dense_switch, preferred_element_type=jnp.float32))
    combined = routed + switch[:, None] * dense_out
    total_square = lax.psum(jnp.sum(combined * combined, axis=1), "tp")
    scale = lax.rsqrt(total_square / width + norm_eps)
    stream_part = lax.dynamic_slice_in_dim(stream, tp_index * quarter, quarter, 1).astype(
        jnp.float32
    )
    layer_out = (stream_part + combined * scale[:, None] * out_gain.astype(jnp.float32)).astype(
        jnp.bfloat16
    )
    new_conv = history[:, :, 1:, :]
    return (layer_out, new_state, new_conv)


def solution(mesh):
    placed = (
        P("ep", None),
        P(),
        P(None, "tp"),
        P(None, "tp"),
        P(None, "tp"),
        P(None, "tp"),
        P(),
        P("tp"),
        P("tp"),
        P(None, None, "tp"),
        P("ep", None, None, "tp"),
        P("ep", "tp", None, None),
        P("tp"),
        P("tp", None),
        P(),
        P(),
        P(),
        P(),
        P("ep", None),
        P("ep", None, "tp"),
        P("ep", None, "tp"),
        P("ep", "tp", None),
        P(),
        P("ep", "tp"),
        P("ep", "tp"),
        P("ep", "tp"),
        P("tp"),
    )
    return jax.shard_map(
        on_device,
        mesh=mesh,
        in_specs=placed,
        out_specs=(P("ep", "tp"), P("ep", "tp", None, None), P("ep", None, None, "tp")),
        check_vma=False,
    )
```

profile of v0, /device:TPU:0, one launch (start us, length us, event | category | flops | bytes accessed | tf_op | source)
XLA Modules:
  0.0 219.6 jit_solution(17043526989973223200)
XLA Ops:
  9.0 1.1 fusion.24
  10.1 1.4 fusion.2
  11.4 1.4 fusion.3
  12.8 1.4 fusion.4
  14.2 0.9 multiply_reduce_fusion.2
  15.3 1.0 fusion.48
  16.7 2.1 multiply_reduce_fusion
  18.9 2.3 %convolution_convert_fusion.3 = bf16[32,2048]{1,0:T(8,128)(2,1)} fusion(bf16[128,2048]{1,0:T(8,128)(2,1)} %param.40, f32[32,128]{1,0:T(8,128)S(1)} %reshape.185, f32[128]{0:T(128)S(1)} %convert_element_type.95, bf16[2048,128]{1,0:T(8,128)(2,1)} %param.30, bf16[32,2048]{1,0:T(8,128)(2,1)S(1)} %copy-done.1, f32[2048]{0:T(1024)S(1)} %convert_element_type.91, ...), kind=kOutput, calls=%fused_computation.5 | convolution fusion | flops 33910784 | bytes 1335936 | tf_op jit(solution)/shard_map/dot_general | solution.py:84
  22.8 33.1 %all-reduce.4.cloned.1.call-done = bf16[32,2048]{1,0:T(8,128)(2,1)} async-done(((bf16[32,2048]{1,0:T(8,128)(2,1)}), bf16[32,2048]{1,0:T(8,128)(2,1)}) %all-reduce.4.cloned.1.call-update) | async-done | bytes 131088 | tf_op jit(solution)/shard_map/psum | solution.py:83
  55.9 1.0 fusion.15
  57.0 1.2 fusion.17
  58.5 0.9 reshape.203
  59.4 2.2 %scatter_custom_fusion = bf16[256,2048]{1,0:T(8,128)(2,1)S(1)} fusion(s32[128]{0:T(128)S(1)} %fusion.39, bf16[128,2048]{1,0:T(8,128)(2,1)} %reshape.203, bf16[]{:T(256)} %constant.57.clone.1), kind=kCustom, calls=%fused_computation.28 | custom fusion | bytes 1049088 | tf_op jit(solution)/shard_map/scatter | solution.py:110
  61.7 36.1 %all_to_all.10 = bf16[8,32,2048]{2,1,0:T(8,128)(2,1)S(1)} all-to-all(bf16[8,32,2048]{2,1,0:T(8,128)(2,1)S(1)} %bitcast.63), channel_id=1, replica_groups=mesh['ep'=8,'tp'=4] {'ep'}, dimensions={0} | all-to-all | bytes 2097152 | tf_op jit(solution)/shard_map/all_to_all | solution.py:112
  98.7 1.4 convolution_convert_fusion
  102.6 3.1 %convolution_convert_fusion.1 = bf16[32,2048]{1,0:T(8,128)(2,1)} fusion(bf16[2048,512]{1,0:T(8,128)(2,1)} %all-gather.6.cloned.1.call-done, bf16[32,2048]{1,0:T(8,128)(2,1)S(1)} %fusion.19, s32[]{:T(128)S(6)} %select_n.38), kind=kOutput, calls=%fused_computation.3 | convolution fusion | flops 67174400 | bytes 2260996 | tf_op jit(solution)/shard_map/sd,cd->sc/dot_general | solution.py:134
  105.7 17.5 %reduce-scatter.2.cloned.1.call-done = bf16[8,32,512]{2,1,0:T(8,128)(2,1)} async-done(((bf16[8,32,2048]{2,1,0:T(8,128)(2,1)}), bf16[8,32,512]{2,1,0:T(8,128)(2,1)}) %reduce-scatter.2.cloned.1.call-update) | async-done | bytes 262160 | tf_op jit(solution)/shard_map/reduce_scatter | solution.py:122
  123.2 5.5 %all-to-all-start.1 = ((bf16[8,32,512]{2,1,0:T(8,128)(2,1)}), bf16[8,32,512]{2,1,0:T(8,128)(2,1)S(1)}, u32[]{:S(2)}, u32[]{:S(2)}) async-start(bf16[8,32,512]{2,1,0:T(8,128)(2,1)} %reduce-scatter.2.cloned.1.call-done), calls=%async_computation.2 | async-start | bytes 524288 | tf_op jit(solution)/shard_map/all_to_all | solution.py:123
  128.8 24.4 %all-gather.4.cloned.1.call-done = bf16[2048,512]{1,0:T(8,128)(2,1)} async-done(((bf16[256,512]{1,0:T(8,128)(2,1)}), bf16[2048,512]{1,0:T(8,128)(2,1)}) %all-gather.4.cloned.1.call-update) | async-done | bytes 2097168 | tf_op jit(solution)/shard_map/all_gather | solution.py:131
  153.2 3.0 %convolution_convert_fusion.2 = bf16[32,2048]{1,0:T(8,128)(2,1)} fusion(bf16[2048,512]{1,0:T(8,128)(2,1)} %all-gather.4.cloned.1.call-done, bf16[32,2048]{1,0:T(8,128)(2,1)S(1)} %fusion.19, s32[]{:T(128)S(6)} %select_n.38), kind=kOutput, calls=%fused_computation.4 | convolution fusion | flops 67174400 | bytes 2260996 | tf_op jit(solution)/shard_map/sd,cd->sc/dot_general | solution.py:128
  156.3 0.8 gather_fusion
  157.5 46.1 %all-gather.8.cloned.1.call-done = bf16[2048,512]{1,0:T(8,128)(2,1)} async-done(((bf16[256,512]{1,0:T(8,128)(2,1)}), bf16[2048,512]{1,0:T(8,128)(2,1)}) %all-gather.8.cloned.1.call-update) | async-done | bytes 2097168 | tf_op jit(solution)/shard_map/all_gather | solution.py:149
  203.6 2.3 %multiply_reduce_fusion.3 = (f32[32]{0:T(128)S(1)}, f32[32,512]{1,0:T(8,128)S(1)}) fusion(f32[32,512]{1,0:T(8,128)S(1)} %multiply_reduce_fusion.1, bf16[2048,512]{1,0:T(8,128)(2,1)} %all-gather.8.cloned.1.call-done, bf16[32,2048]{1,0:T(8,128)(2,1)} %get-tuple-element.3, bf16[32,2048]{1,0:T(8,128)(2,1)} %get-tuple-element.4, f32[32]{0:T(128)S(1)} %fusion.8), kind=kOutput, calls=%fused_computation.58 | convolution fusion | flops 67698656 | bytes 2490624 | tf_op jit(solution)/shard_map/dot_general | solution.py:147
  205.9 5.7 %psum.31 = f32[32]{0:T(128)S(1)} all-reduce(f32[32]{0:T(128)S(1)} %get-tuple-element.18), channel_id=1, replica_groups=mesh['ep'=8,'tp'=4] {'tp'}, use_global_device_ids=true, to_apply=%region_18.19 | all-reduce | flops 32 | bytes 256 | tf_op jit(solution)/shard_map/psum | solution.py:154
  (94 shorter events, 7.8 us)
Async XLA Ops:
  8.0 90.7 %copy-start = (bf16[1,256,2048]{2,1,0:T(8,128)(2,1)S(1)}, bf16[1,256,2048]{2,1,0:T(8,128)(2,1)}, u32[]{:S(2)}) copy-start(bf16[1,256,2048]{2,1,0:T(8,128)(2,1)} %param.48) | copy-start | bytes 3145732
  8.0 7.3 %copy-start.1 = (bf16[32,2048]{1,0:T(8,128)(2,1)S(1)}, bf16[32,2048]{1,0:T(8,128)(2,1)}, u32[]{:S(2)}) copy-start(bf16[32,2048]{1,0:T(8,128)(2,1)} %param.27) | copy-start | bytes 393220
  8.0 6.2 %copy-start.9 = (bf16[3,4,128]{2,1,0:T(4,128)(2,1)S(1)}, bf16[3,4,128]{2,1,0:T(4,128)(2,1)}, u32[]{:S(2)}) copy-start(bf16[3,4,128]{2,1,0:T(4,128)(2,1)} %param.36) | copy-start | bytes 9220
  8.0 8.2 %copy-start.14 = (f32[2]{0:T(128)S(1)}, f32[2]{0:T(128)}, u32[]{:S(2)}) copy-start(f32[2]{0:T(128)} %param.35) | copy-start | bytes 28
  8.0 8.2 %copy-start.11 = (f32[2]{0:T(128)S(1)}, f32[2]{0:T(128)}, u32[]{:S(2)}) copy-start(f32[2]{0:T(128)} %param.34) | copy-start | bytes 28
  8.1 8.6 %copy-start.2 = (f32[32,2,64,128]{3,2,1,0:T(8,128)S(1)}, f32[32,2,64,128]{3,2,1,0:T(8,128)}, u32[]{:S(2)}) copy-start(f32[32,2,64,128]{3,2,1,0:T(8,128)} %param.38) | copy-start | bytes 6291460
  8.1 47.9 %all-reduce.4.cloned.1.call-start = ((), (), s32[]{:S(2)}) async-start(), calls=%async_computation.3 | async-start | bytes 262144 | tf_op jit(solution)/shard_map/psum | solution.py:83
  16.7 2.2 %copy-start.15 = (bf16[128]{0:T(256)(128)(2,1)S(1)}, bf16[128]{0:T(256)(128)(2,1)}, u32[]{:S(2)}) copy-start(bf16[128]{0:T(256)(128)(2,1)} %param.39) | copy-start | bytes 772
  16.7 5.2 %copy-start.5 = (s32[32,4]{0,1:T(4,128)S(1)}, s32[32,4]{0,1:T(4,128)}, u32[]{:S(2)}) copy-start(s32[32,4]{0,1:T(4,128)} %param.45) | copy-start | bytes 1540
  16.7 5.3 %copy-start.6 = (bf16[2048]{0:T(1024)(128)(2,1)S(1)}, bf16[2048]{0:T(1024)(128)(2,1)}, u32[]{:S(2)}) copy-start(bf16[2048]{0:T(1024)(128)(2,1)} %param.41) | copy-start | bytes 12292
  16.7 5.3 %copy-start.7 = (bf16[2048]{0:T(1024)(128)(2,1)S(1)}, bf16[2048]{0:T(1024)(128)(2,1)}, u32[]{:S(2)}) copy-start(bf16[2048]{0:T(1024)(128)(2,1)} %param.42) | copy-start | bytes 12292
  21.3 81.3 %all-gather.6.cloned.1.call-start = ((), (), s32[]{:S(2)}) async-start(), calls=%async_computation.6 | async-start | bytes 2359296 | tf_op jit(solution)/shard_map/all_gather | solution.py:137
  21.9 101.4 %reduce-scatter.2.cloned.1.call-start = ((), (), s32[]{:S(2)}) async-start(), calls=%async_computation.4 | async-start | bytes 1310720 | tf_op jit(solution)/shard_map/reduce_scatter | solution.py:122
  58.5 39.2 %copy-start.3 = (bf16[1,2048,256]{2,1,0:T(8,128)(2,1)S(1)}, bf16[1,2048,256]{2,1,0:T(8,128)(2,1)}, u32[]{:S(2)}) copy-start(bf16[1,2048,256]{2,1,0:T(8,128)(2,1)} %param.46) | copy-start | bytes 3145732
  61.6 36.5 %copy-start.12 = (bf16[1,2048,256]{2,1,0:T(8,128)(2,1)S(1)}, bf16[1,2048,256]{2,1,0:T(8,128)(2,1)}, u32[]{:S(2)}) copy-start(bf16[1,2048,256]{2,1,0:T(8,128)(2,1)} %param.47) | copy-start | bytes 3145732
  98.6 2.7 %copy-start.8 = (bf16[2048]{0:T(1024)(128)(2,1)S(1)}, bf16[2048]{0:T(1024)(128)(2,1)}, u32[]{:S(2)}) copy-start(bf16[2048]{0:T(1024)(128)(2,1)} %param.49) | copy-start | bytes 12292
  98.6 2.7 %copy-start.10 = (bf16[512]{0:T(512)(128)(2,1)S(1)}, bf16[512]{0:T(512)(128)(2,1)}, u32[]{:S(2)}) copy-start(bf16[512]{0:T(512)(128)(2,1)} %param.53) | copy-start | bytes 3076
  98.7 3.4 %copy-start.4 = (bf16[2048,8]{0,1:T(8,128)(2,1)S(1)}, bf16[2048,8]{0,1:T(8,128)(2,1)}, u32[]{:S(2)}) copy-start(bf16[2048,8]{0,1:T(8,128)(2,1)} %param.44) | copy-start | bytes 98308
  98.7 3.6 %copy-start.13 = (bf16[2048,2]{0,1:T(2,128)(2,1)S(1)}, bf16[2048,2]{0,1:T(2,128)(2,1)}, u32[]{:S(2)}) copy-start(bf16[2048,2]{0,1:T(2,128)(2,1)} %param.43) | copy-start | bytes 24580
  100.2 53.1 %all-gather.4.cloned.1.call-start = ((), (), s32[]{:S(2)}) async-start(), calls=%async_computation.5 | async-start | bytes 2359296 | tf_op jit(solution)/shard_map/all_gather | solution.py:131
  100.7 102.8 %all-gather.8.cloned.1.call-start = ((), (), s32[]{:S(2)}) async-start(), calls=%async_computation.7 | async-start | bytes 2359296 | tf_op jit(solution)/shard_map/all_gather | solution.py:149
  123.2 33.1 %all-to-all-start.1 = ((bf16[8,32,512]{2,1,0:T(8,128)(2,1)}), bf16[8,32,512]{2,1,0:T(8,128)(2,1)S(1)}, u32[]{:S(2)}, u32[]{:S(2)}) async-start(bf16[8,32,512]{2,1,0:T(8,128)(2,1)} %reduce-scatter.2.cloned.1.call-done), calls=%async_computation.2 | async-start | bytes 524288 | tf_op jit(solution)/shard_map/all_to_all | solution.py:123
  128.8 74.8 %all-reduce.6.cloned.1.call-start = ((), (), s32[]{:S(2)}) async-start(), calls=%async_computation.8 | async-start | bytes 524288 | tf_op jit(solution)/shard_map/psum | solution.py:144
Sparse Core Ops, SparseCore 0:
  21.4 34.4 all-reduce.3
  100.3 22.9 reduce-scatter.1
  156.3 31.6 all-reduce.5
Sparse Core Ops, SparseCore 1:
  23.9 59.7 all-gather.5
  102.8 50.4 all-gather.3
  155.2 48.3 all-gather.7
where the time goes:
time: 220 us
  waiting for transfers between devices  123 us (56%)
  blocking collectives  41.7 us (19%)
  matrix products  18.6 us (8%)
  between operations  15.9 us (7%)
  other arithmetic  8.99 us (4%)
  local copies, waits for them, and re-layouts  5.86 us (3%)
  starting transfers between devices  5.78 us (3%)
    all_gather x1, waiting for transfers between devices, on_device(): lax.all_gather(dense_down, 'ep', axis=0, tiled=True)  46.1 us
    all_to_all x1, blocking collectives, on_device(): lax.all_to_all(outgoing, 'ep', split_axis=0, concat_axis=0, tiled=True)  36.1 us
    psum x1, waiting for transfers between devices, on_device(): lax.psum(jnp.dot(gated, proj_out, preferred_element_type=jnp.float32).ast...  33.1 us
    all_gather x1, waiting for transfers between devices, on_device(): lax.all_gather(dense_gate, 'ep', axis=0, tiled=True)  24.4 us
    reduce_scatter x1, waiting for transfers between devices, on_device(): lax.psum_scatter(result.astype(jnp.bfloat16), 'tp', scatter_dimension=2,...  17.5 us
    psum x1, blocking collectives, on_device(): total_square = lax.psum(jnp.sum(combined * combined, axis=1), 'tp')  5.67 us
    all_to_all x1, starting transfers between devices, on_device(): lax.all_to_all(summed, 'ep', split_axis=0, concat_axis=0, tiled=True)  5.53 us
  transfers between devices with their start and end apart: 7, of which 4 were waited for; matrix products, arithmetic and copies ran while one was open for 8% of the time, Pallas kernels for 0%

commit v1 on v0

--- a/solution.py
+++ b/solution.py
@@ -80,8 +80,11 @@
     new_state = keep[:, :, None, None] * scan_state + driven[:, :, :, None] * b_heads[:, :, None, :]
     read = jnp.sum(new_state * c_heads[:, :, None, :], axis=3).reshape(seqs, channels)
     gated = (read * jax.nn.silu(gate_z) * inner_gain.astype(jnp.float32)).astype(jnp.bfloat16)
-    mixed = lax.psum(
-        jnp.dot(gated, proj_out, preferred_element_type=jnp.float32).astype(jnp.bfloat16), "tp"
+    mixed = jnp.sum(
+        lax.all_gather(
+            jnp.dot(gated, proj_out, preferred_element_type=jnp.float32).astype(jnp.bfloat16), "tp"
+        ),
+        axis=0,
     ).astype(jnp.float32)
     stream = (resid.astype(jnp.float32) + scaled_rows(mixed, post_gain)).astype(jnp.bfloat16)
     feed = scaled_rows(stream, ffn_gain).astype(jnp.bfloat16)

time: 220 us -> 240 us (1.091)
  waiting for transfers between devices: 123 us -> 139 us
  blocking collectives: 41.7 us -> 46.3 us
    psum x1 -> x0, waiting for transfers between devices: 33.1 us -> none  [on_device(): lax.psum(jnp.dot(gated, proj_out, preferred_element_type=jnp.float32).ast...]
    all_gather x1, waiting for transfers between devices: 0.01 us -> 24.4 us  [on_device(): lax.all_gather(dense_up, 'ep', axis=0, tiled=True)]
    all_gather x1, waiting for transfers between devices: 24.4 us -> 47.4 us  [on_device(): lax.all_gather(dense_gate, 'ep', axis=0, tiled=True)]
    all_gather x0 -> x1, blocking collectives: none -> 8.65 us  [on_device(): lax.all_gather(jnp.dot(gated, proj_out, preferred_element_type=jnp.float3...]
    all_to_all x1, blocking collectives: 36.1 us -> 32 us  [on_device(): lax.all_to_all(outgoing, 'ep', split_axis=0, concat_axis=0, tiled=True)]
    reduce_scatter x1, waiting for transfers between devices: 17.5 us -> 21.2 us  [on_device(): lax.psum_scatter(result.astype(jnp.bfloat16), 'tp', scatter_dimension=2,...]
  transfers between devices with their start and end apart: 7 -> 6, of which waited for: 4 -> 4; matrix products, arithmetic and copies ran while one was open for 8% -> 3% of each run, Pallas kernels for 0% -> 0%
where the time goes in v1:
time: 240 us
  waiting for transfers between devices  139 us (58%)
  blocking collectives  46.3 us (19%)
  matrix products  17.7 us (7%)
  between operations  16.1 us (7%)
  other arithmetic  7.76 us (3%)
  local copies, waits for them, and re-layouts  6.69 us (3%)
  starting transfers between devices  5.72 us (2%)
    all_gather x1, waiting for transfers between devices, on_device(): lax.all_gather(dense_gate, 'ep', axis=0, tiled=True)  47.4 us
    all_gather x1, waiting for transfers between devices, on_device(): lax.all_gather(dense_down, 'ep', axis=0, tiled=True)  44.7 us
    all_to_all x1, blocking collectives, on_device(): lax.all_to_all(outgoing, 'ep', split_axis=0, concat_axis=0, tiled=True)  32 us
    all_gather x1, waiting for transfers between devices, on_device(): lax.all_gather(dense_up, 'ep', axis=0, tiled=True)  24.4 us
    reduce_scatter x1, waiting for transfers between devices, on_device(): lax.psum_scatter(result.astype(jnp.bfloat16), 'tp', scatter_dimension=2,...  21.2 us
    all_gather x1, blocking collectives, on_device(): lax.all_gather(jnp.dot(gated, proj_out, preferred_element_type=jnp.float3...  8.65 us
    psum x1, blocking collectives, on_device(): total_square = lax.psum(jnp.sum(combined * combined, axis=1), 'tp')  5.67 us
    all_to_all x1, starting transfers between devices, on_device(): lax.all_to_all(summed, 'ep', split_axis=0, concat_axis=0, tiled=True)  5.51 us
  transfers between devices with their start and end apart: 6, of which 4 were waited for; matrix products, arithmetic and copies ran while one was open for 3% of the time, Pallas kernels for 0%

profile of v1, /device:TPU:0, one launch (start us, length us, event | category | flops | bytes accessed | tf_op | source)
XLA Modules:
  0.0 239.6 jit_solution(16604459808767391345)
XLA Ops:
  8.1 0.9 copy.45
  10.4 1.0 fusion.24
  11.5 1.4 fusion.2
  12.9 1.4 fusion.3
  14.3 1.4 fusion.4
  15.7 0.9 multiply_reduce_fusion.2
  16.7 1.0 fusion.48
  18.1 2.1 multiply_reduce_fusion
  20.3 1.7 convolution_convert_fusion.3
  22.0 8.7 %all-gather = bf16[128,2048]{1,0:T(8,128)(2,1)S(1)} all-gather(bf16[32,2048]{1,0:T(8,128)(2,1)S(1)} %convolution_convert_fusion.3), channel_id=2, replica_groups=mesh['ep'=8,'tp'=4] {'tp'}, dimensions={0}, use_global_device_ids=true | all-gather | bytes 655360 | tf_op jit(solution)/shard_map/all_gather | solution.py:84
  31.5 0.9 reshape.203
  33.2 2.2 scatter_custom_fusion
  35.4 32.0 %all_to_all.10 = bf16[8,32,2048]{2,1,0:T(8,128)(2,1)S(1)} all-to-all(bf16[8,32,2048]{2,1,0:T(8,128)(2,1)S(1)} %bitcast.64), channel_id=1, replica_groups=mesh['ep'=8,'tp'=4] {'ep'}, dimensions={0} | all-to-all | bytes 2097152 | tf_op jit(solution)/shard_map/all_to_all | solution.py:115
  68.4 1.4 convolution_convert_fusion
  72.2 21.2 %reduce-scatter.2.cloned.1.call-done = bf16[8,32,512]{2,1,0:T(8,128)(2,1)} async-done(((bf16[8,32,2048]{2,1,0:T(8,128)(2,1)}), bf16[8,32,512]{2,1,0:T(8,128)(2,1)}) %reduce-scatter.2.cloned.1.call-update) | async-done | bytes 262160 | tf_op jit(solution)/shard_map/reduce_scatter | solution.py:125
  93.5 5.5 %all-to-all-start.1 = ((bf16[8,32,512]{2,1,0:T(8,128)(2,1)}), bf16[8,32,512]{2,1,0:T(8,128)(2,1)S(1)}, u32[]{:S(2)}, u32[]{:S(2)}) async-start(bf16[8,32,512]{2,1,0:T(8,128)(2,1)} %reduce-scatter.2.cloned.1.call-done), calls=%async_computation.2 | async-start | bytes 524288 | tf_op jit(solution)/shard_map/all_to_all | solution.py:126
  99.0 24.4 %all-gather.7.cloned.1.call-done = bf16[2048,512]{1,0:T(8,128)(2,1)} async-done(((bf16[256,512]{1,0:T(8,128)(2,1)}), bf16[2048,512]{1,0:T(8,128)(2,1)}) %all-gather.7.cloned.1.call-update) | async-done | bytes 2097168 | tf_op jit(solution)/shard_map/all_gather | solution.py:140
  123.5 3.0 %convolution_convert_fusion.1 = bf16[32,2048]{1,0:T(8,128)(2,1)} fusion(bf16[2048,512]{1,0:T(8,128)(2,1)} %all-gather.7.cloned.1.call-done, bf16[32,2048]{1,0:T(8,128)(2,1)S(1)} %fusion.19, s32[]{:T(128)S(6)} %select_n.38), kind=kOutput, calls=%fused_computation.3 | convolution fusion | flops 67174400 | bytes 2260996 | tf_op jit(solution)/shard_map/sd,cd->sc/dot_general | solution.py:137
  126.4 47.4 %all-gather.5.cloned.1.call-done = bf16[2048,512]{1,0:T(8,128)(2,1)} async-done(((bf16[256,512]{1,0:T(8,128)(2,1)}), bf16[2048,512]{1,0:T(8,128)(2,1)}) %all-gather.5.cloned.1.call-update) | async-done | bytes 2097168 | tf_op jit(solution)/shard_map/all_gather | solution.py:134
  173.8 3.0 %convolution_convert_fusion.2 = bf16[32,2048]{1,0:T(8,128)(2,1)} fusion(bf16[2048,512]{1,0:T(8,128)(2,1)} %all-gather.5.cloned.1.call-done, bf16[32,2048]{1,0:T(8,128)(2,1)S(1)} %fusion.19, s32[]{:T(128)S(6)} %select_n.38), kind=kOutput, calls=%fused_computation.4 | convolution fusion | flops 67174400 | bytes 2260996 | tf_op jit(solution)/shard_map/sd,cd->sc/dot_general | solution.py:131
  177.5 0.8 gather_fusion
  178.7 44.7 %all-gather.9.cloned.1.call-done = bf16[2048,512]{1,0:T(8,128)(2,1)} async-done(((bf16[256,512]{1,0:T(8,128)(2,1)}), bf16[2048,512]{1,0:T(8,128)(2,1)}) %all-gather.9.cloned.1.call-update) | async-done | bytes 2097168 | tf_op jit(solution)/shard_map/all_gather | solution.py:152
  223.4 2.3 multiply_reduce_fusion.3
  225.7 5.7 %psum.23 = f32[32]{0:T(128)S(1)} all-reduce(f32[32]{0:T(128)S(1)} %get-tuple-element.18), channel_id=1, replica_groups=mesh['ep'=8,'tp'=4] {'tp'}, use_global_device_ids=true, to_apply=%region_18.19 | all-reduce | flops 32 | bytes 256 | tf_op jit(solution)/shard_map/psum | solution.py:157
  (93 shorter events, 8.6 us)
Async XLA Ops:
  8.0 60.4 %copy-start = (bf16[1,256,2048]{2,1,0:T(8,128)(2,1)S(1)}, bf16[1,256,2048]{2,1,0:T(8,128)(2,1)}, u32[]{:S(2)}) copy-start(bf16[1,256,2048]{2,1,0:T(8,128)(2,1)} %param.48) | copy-start | bytes 3145732
  8.0 8.7 %copy-start.1 = (bf16[32,2048]{1,0:T(8,128)(2,1)S(1)}, bf16[32,2048]{1,0:T(8,128)(2,1)}, u32[]{:S(2)}) copy-start(bf16[32,2048]{1,0:T(8,128)(2,1)} %param.27) | copy-start | bytes 393220
  8.0 7.6 %copy-start.9 = (bf16[3,4,128]{2,1,0:T(4,128)(2,1)S(1)}, bf16[3,4,128]{2,1,0:T(4,128)(2,1)}, u32[]{:S(2)}) copy-start(bf16[3,4,128]{2,1,0:T(4,128)(2,1)} %param.36) | copy-start | bytes 9220
  8.0 9.7 %copy-start.14 = (f32[2]{0:T(128)S(1)}, f32[2]{0:T(128)}, u32[]{:S(2)}) copy-start(f32[2]{0:T(128)} %param.35) | copy-start | bytes 28
  8.0 9.7 %copy-start.11 = (f32[2]{0:T(128)S(1)}, f32[2]{0:T(128)}, u32[]{:S(2)}) copy-start(f32[2]{0:T(128)} %param.34) | copy-start | bytes 28
  8.1 10.1 %copy-start.2 = (f32[32,2,64,128]{3,2,1,0:T(8,128)S(1)}, f32[32,2,64,128]{3,2,1,0:T(8,128)}, u32[]{:S(2)}) copy-start(f32[32,2,64,128]{3,2,1,0:T(8,128)} %param.38) | copy-start | bytes 6291460
  8.1 85.4 %reduce-scatter.2.cloned.1.call-start = ((), (), s32[]{:S(2)}) async-start(), calls=%async_computation.3 | async-start | bytes 1310720 | tf_op jit(solution)/shard_map/reduce_scatter | solution.py:125
  18.1 2.2 copy-start.15
  20.2 10.7 %copy-start.6 = (bf16[2048]{0:T(1024)(128)(2,1)S(1)}, bf16[2048]{0:T(1024)(128)(2,1)}, u32[]{:S(2)}) copy-start(bf16[2048]{0:T(1024)(128)(2,1)} %param.41) | copy-start | bytes 12292
  20.2 10.9 %copy-start.7 = (bf16[2048]{0:T(1024)(128)(2,1)S(1)}, bf16[2048]{0:T(1024)(128)(2,1)}, u32[]{:S(2)}) copy-start(bf16[2048]{0:T(1024)(128)(2,1)} %param.42) | copy-start | bytes 12292
  31.5 35.9 %copy-start.3 = (bf16[1,2048,256]{2,1,0:T(8,128)(2,1)S(1)}, bf16[1,2048,256]{2,1,0:T(8,128)(2,1)}, u32[]{:S(2)}) copy-start(bf16[1,2048,256]{2,1,0:T(8,128)(2,1)} %param.46) | copy-start | bytes 3145732
  35.4 32.5 %copy-start.12 = (bf16[1,2048,256]{2,1,0:T(8,128)(2,1)S(1)}, bf16[1,2048,256]{2,1,0:T(8,128)(2,1)}, u32[]{:S(2)}) copy-start(bf16[1,2048,256]{2,1,0:T(8,128)(2,1)} %param.47) | copy-start | bytes 3145732
  68.3 3.3 %copy-start.8 = (bf16[2048]{0:T(1024)(128)(2,1)S(1)}, bf16[2048]{0:T(1024)(128)(2,1)}, u32[]{:S(2)}) copy-start(bf16[2048]{0:T(1024)(128)(2,1)} %param.49) | copy-start | bytes 12292
  68.4 3.3 %copy-start.4 = (bf16[2048,8]{0,1:T(8,128)(2,1)S(1)}, bf16[2048,8]{0,1:T(8,128)(2,1)}, u32[]{:S(2)}) copy-start(bf16[2048,8]{0,1:T(8,128)(2,1)} %param.44) | copy-start | bytes 98308
  68.4 3.4 %copy-start.5 = (s32[32,4]{0,1:T(4,128)S(1)}, s32[32,4]{0,1:T(4,128)}, u32[]{:S(2)}) copy-start(s32[32,4]{0,1:T(4,128)} %param.45) | copy-start | bytes 1540
  68.4 3.5 %copy-start.13 = (bf16[2048,2]{0,1:T(2,128)(2,1)S(1)}, bf16[2048,2]{0,1:T(2,128)(2,1)}, u32[]{:S(2)}) copy-start(bf16[2048,2]{0,1:T(2,128)(2,1)} %param.43) | copy-start | bytes 24580
  69.9 53.6 %all-gather.7.cloned.1.call-start = ((), (), s32[]{:S(2)}) async-start(), calls=%async_computation.5 | async-start | bytes 2359296 | tf_op jit(solution)/shard_map/all_gather | solution.py:140
  70.5 103.4 %all-gather.5.cloned.1.call-start = ((), (), s32[]{:S(2)}) async-start(), calls=%async_computation.4 | async-start | bytes 2359296 | tf_op jit(solution)/shard_map/all_gather | solution.py:134
  71.0 152.4 %all-gather.9.cloned.1.call-start = ((), (), s32[]{:S(2)}) async-start(), calls=%async_computation.6 | async-start | bytes 2359296 | tf_op jit(solution)/shard_map/all_gather | solution.py:152
  93.5 84.1 %all-to-all-start.1 = ((bf16[8,32,512]{2,1,0:T(8,128)(2,1)}), bf16[8,32,512]{2,1,0:T(8,128)(2,1)S(1)}, u32[]{:S(2)}, u32[]{:S(2)}) async-start(bf16[8,32,512]{2,1,0:T(8,128)(2,1)} %reduce-scatter.2.cloned.1.call-done), calls=%async_computation.2 | async-start | bytes 524288 | tf_op jit(solution)/shard_map/all_to_all | solution.py:126
  99.0 77.9 %copy-start.10 = (bf16[512]{0:T(512)(128)(2,1)S(1)}, bf16[512]{0:T(512)(128)(2,1)}, u32[]{:S(2)}) copy-start(bf16[512]{0:T(512)(128)(2,1)} %param.53) | copy-start | bytes 3076
  99.0 124.4 %all-reduce.3.cloned.1.call-start = ((), (), s32[]{:S(2)}) async-start(), calls=%async_computation.7 | async-start | bytes 524288 | tf_op jit(solution)/shard_map/psum | solution.py:147
Sparse Core Ops, SparseCore 0:
  70.0 23.4 reduce-scatter.1
  176.9 30.9 all-reduce.2
Sparse Core Ops, SparseCore 1:
  72.5 50.9 all-gather.6
  125.5 48.3 all-gather.4
  175.8 47.5 all-gather.8
